TPU v7x, 32 devices: a whole 2x2x4 slice. The times are simulated.
32 devices in a mesh: sp: 8 (over z, core), tp: 4 (over y, x).
Axes of the slice: x: 2, y: 2, z: 4, core: 2. Of those that a mesh axis runs over, the one named last changes fastest.
Arguments:
- tokens: bfloat16 [2, 6144, 4096], P(None, 'sp', 'tp'), may hold values from -6 to 6
- w_key: bfloat16 [4096, 2048], P(None, 'tp'), may hold values from -0.09375 to 0.09375
- w_value: bfloat16 [4096, 2048], P(None, 'tp'), may hold values from -0.09375 to 0.09375
- w_gate: bfloat16 [4096, 4, 16], replicated, may hold values from -0.09375 to 0.09375
- forget_bias: float32 [2, 16], replicated, may hold values from 3.9 to 13, as said below
- log_shift: float32 [2, 4, 16, 6144], P(None, None, 'tp', 'sp'), may hold values from -5 to 121, as said below
- new_query: bfloat16 [2, 1024, 2048], P(None, 'sp', 'tp'), may hold values from -6 to 6
Outputs:
- cache_matrix: bfloat16 [2, 2, 16, 128, 128], P(None, None, 'tp')
- cache_norm: float32 [2, 2, 16, 128], P(None, None, 'tp')
- cache_max: float32 [2, 2, 16], P(None, None, 'tp')
- first_read: bfloat16 [2, 1024, 2048], P(None, 'sp', 'tp')
Inputs may be any that keep to these rules, and one draw needn't show every extreme that they name: `forget_bias`: added to the forget gates' pre-activations, by direction and head. `log_shift`: rows 0 and 2 are added to the input gates of the two directions; rows 1 and 3 are added to the log forget gates and are never positive.
All inputs are finite; a program needn't handle non-finite values.
Results may differ from a plain program's by a relative error of at most 0.024.
Values may be sent and summed in bfloat16 or wider, within the bound.
No kernel may reach another device: no remote copies, remote signals or barrier semaphores. Data moves between devices by JAX's collectives and lax.ppermute only.
A program may use at most 64 MiB of HBM per device.

v0:
```python
import jax
import jax.numpy as jnp
from jax import lax
from jax.sharding import PartitionSpec as P

HEAD = 128


def combined_all(array, axis, combine):
    everything = jax.tree.map(lambda part: lax.all_gather(part, axis), array)
    leading = jax.tree.map(lambda part: part[0], everything)

    def lap(k, so_far):
        return combine(so_far, jax.tree.map(lambda part: part[k], everything))

    return lax.fori_loop(1, lax.axis_size(axis), lap, leading)


def joint_max(earlier, latter):
    memory_a, norm_a, high_a = earlier
    memory_b, norm_b, high_b = latter
    highest = jnp.maximum(high_a, high_b)
    carried = jnp.exp(high_a - highest)
    own_part = jnp.exp(high_b - highest)
    memory = memory_a * carried[..., None, None] + memory_b * own_part[..., None, None]
    norm_sum = norm_a * carried[..., None] + norm_b * own_part[..., None]
    return (memory, norm_sum, highest)


def on_device(tokens, w_key, w_value, w_gate, forget_bias, log_shift, new_query):
    seq_count, seg_len, part_width = tokens.shape
    per_head = w_key.shape[1] // HEAD
    row_count = seq_count * seg_len
    first_head = lax.axis_index("tp") * per_head
    gate_cols = lax.dynamic_slice_in_dim(w_gate, first_head, per_head, 2).reshape(
        w_gate.shape[0], 4 * per_head
    )
    bias_own = lax.dynamic_slice_in_dim(forget_bias, first_head, per_head, 1)
    piece = lax.all_gather(tokens, "tp", axis=2, tiled=True)
    piece_width = piece.shape[2]
    flat_piece = piece.reshape(row_count, piece_width)
    key_sum = jnp.dot(flat_piece, w_key, preferred_element_type=jnp.float32)
    value_sum = jnp.dot(flat_piece, w_value, preferred_element_type=jnp.float32)
    gate_sum = jnp.dot(flat_piece, gate_cols, preferred_element_type=jnp.float32)
    key_rows = key_sum.astype(jnp.bfloat16).reshape(seq_count, seg_len, per_head, HEAD)
    value_rows = value_sum.astype(jnp.bfloat16).reshape(seq_count, seg_len, per_head, HEAD)
    gates = gate_sum.reshape(seq_count, seg_len, 4, per_head).transpose(0, 2, 3, 1)
    input_fwd = gates[:, 0] + log_shift[:, 0]
    forget_fwd = jax.nn.log_sigmoid(gates[:, 1] + bias_own[0][None, :, None]) + log_shift[:, 1]
    input_bwd = gates[:, 2] + log_shift[:, 2]
    forget_bwd = jax.nn.log_sigmoid(gates[:, 3] + bias_own[1][None, :, None]) + log_shift[:, 3]
    climb_fwd = jnp.cumsum(forget_fwd, axis=-1)
    total_fwd = climb_fwd[..., -1]
    weight_fwd = total_fwd[..., None] - climb_fwd + input_fwd
    climb_bwd = jnp.cumsum(forget_bwd, axis=-1)
    total_bwd = climb_bwd[..., -1]
    weight_bwd = climb_bwd - forget_bwd + input_bwd
    weights = jnp.stack([weight_fwd, weight_bwd], axis=1)
    totals = jnp.stack([total_fwd, total_bwd], axis=1)
    local_top = jnp.max(weights, axis=-1)
    scale_now = jnp.exp(weights - local_top[..., None])
    key_f = key_rows.astype(jnp.float32).transpose(0, 2, 1, 3) * HEAD ** (-0.5)
    value_f = value_rows.astype(jnp.float32).transpose(0, 2, 1, 3)
    weighted = scale_now[..., None] * key_f[:, None]
    memory = jnp.einsum("bjhld,bhle->bjhde", weighted, value_f, precision=lax.Precision.HIGHEST)
    norm_sum = jnp.sum(weighted, axis=3)
    every_total = lax.all_gather(totals[None], "sp", axis=0, tiled=True)
    my_index = lax.axis_index("sp")
    sources = jnp.arange(every_total.shape[0])[:, None, None, None]
    direction = jnp.arange(2)[None, None, :, None]
    counted = jnp.where(direction == 0, sources > my_index, sources < my_index)
    passed = jnp.sum(jnp.where(counted, every_total, 0.0), axis=0)
    total_all = jnp.sum(every_total, axis=0)
    memory_all, norm_all, top_all = combined_all(
        (memory, norm_sum, local_top + passed), "sp", joint_max
    )
    cache_max = jnp.maximum(total_all, top_all)
    rescale = jnp.exp(top_all - cache_max)
    cache_matrix = (memory_all * rescale[..., None, None]).astype(jnp.bfloat16)
    cache_norm = norm_all * rescale[..., None]
    new_count = new_query.shape[1]
    queries = new_query.reshape(seq_count, new_count, per_head, HEAD)
    numerator = jnp.einsum(
        "bthd,bjhde->bjthe", queries, cache_matrix, preferred_element_type=jnp.float32
    )
    denominator = jnp.einsum(
        "bthd,bjhd->bjth", queries.astype(jnp.float32), cache_norm, precision=lax.Precision.HIGHEST
    )
    divisor = jnp.maximum(jnp.abs(denominator), 1.0)
    first_read = jnp.sum(numerator / divisor[..., None], axis=1)
    first_read = first_read.reshape(seq_count, new_count, per_head * HEAD).astype(jnp.bfloat16)
    return (cache_matrix, cache_norm, cache_max, first_read)


def solution(mesh):
    return jax.shard_map(
        on_device,
        mesh=mesh,
        in_specs=(
            P(None, "sp", "tp"),
            P(None, "tp"),
            P(None, "tp"),
            P(),
            P(),
            P(None, None, "tp", "sp"),
            P(None, "sp", "tp"),
        ),
        out_specs=(
            P(None, None, "tp", None, None),
            P(None, None, "tp", None),
            P(None, None, "tp"),
            P(None, "sp", "tp"),
        ),
        check_vma=False,
    )
```

profile of v0, /device:TPU:0, one launch (start us, length us, event | category | flops | bytes accessed | tf_op | source)
XLA Modules:
  0.0 296.8 jit_solution(11978005785362571793)
XLA Ops:
  7.2 0.7 all-gather.7.cloned.1.call-update
  8.0 0.8 fusion.34
  8.9 0.8 constant_dynamic-slice_fusion
  9.7 125.3 %all-gather.7.cloned.1.call-done = bf16[2,768,4096]{2,1,0:T(8,128)(2,1)} async-done(((bf16[2,768,1024]{2,1,0:T(8,128)(2,1)}), bf16[2,768,4096]{2,1,0:T(8,128)(2,1)}) %all-gather.7.cloned.1.call-update) | async-done | bytes 12582928 | tf_op jit(solution)/shard_map/all_gather | solution.py:39
  135.0 7.9 %convolution_bitcast_fusion = f32[1536,16]{0,1:T(8,128)S(1)} fusion(bf16[4096,16]{0,1:T(8,128)(2,1)S(1)} %reshape.198, bf16[1536,4096]{1,0:T(8,128)(2,1)} %bitcast.91), kind=kOutput, calls=%fused_computation.16 | convolution fusion | flops 201326592 | bytes 12812288 | tf_op jit(solution)/shard_map/dot_general | solution.py:44
  143.1 0.1 fusion.22
  143.2 2.3 reduce-window.14
  145.5 0.2 slice_reduce_fusion.1
  145.7 0.4 reduce-window.15
  146.2 0.2 slice_reduce_fusion.3
  146.3 2.3 reduce-window.16
  148.6 0.2 slice_reduce_fusion
  148.7 0.4 reduce-window.19
  149.2 0.1 fusion.30
  149.3 0.1 fusion.25
  149.4 0.1 subtract_exponential_fusion.1
  149.6 11.9 %convolution_convert_fusion.1 = bf16[1536,512]{1,0:T(8,128)(2,1)} fusion(bf16[1536,4096]{1,0:T(8,128)(2,1)} %bitcast.92, bf16[4096,512]{1,0:T(8,128)(2,1)} %param.11), kind=kOutput, calls=%fused_computation.15 | convolution fusion | flops 6443237376 | bytes 18350080 | tf_op jit(solution)/shard_map/dot_general | solution.py:43
  161.5 10.8 %convert_multiply_fusion = f32[1536,512]{1,0:T(8,128)} fusion(bf16[1536,4096]{1,0:T(8,128)(2,1)} %bitcast.93, bf16[4096,512]{1,0:T(8,128)(2,1)S(1)} %copy-done.5), kind=kOutput, calls=%fused_computation.12 | convolution fusion | flops 6444810240 | bytes 19922944 | tf_op jit(solution)/shard_map/dot_general | solution.py:42
  172.2 4.9 %mul.152 = f32[2,768,4,128]{3,2,1,0:T(4,128)} reshape(f32[1536,512]{1,0:T(8,128)} %convert_multiply_fusion) | data formatting | bytes 6291456 | tf_op jit(solution)/shard_map/mul | solution.py:62
  177.1 3.8 %copy.65 = f32[2,4,768,128]{3,2,1,0:T(8,128)} copy(f32[2,4,768,128]{3,1,2,0:T(4,128)} %bitcast.94) | data formatting | bytes 6291456 | tf_op jit(solution)/shard_map/mul | solution.py:62
  180.9 2.4 reshape.197
  183.3 2.3 copy.59
  185.6 5.3 %fusion.8 = f32[2,2,4,128,128]{3,4,1,2,0:T(8,128)S(1)} fusion(f32[2,4,768,128]{3,2,1,0:T(8,128)} %copy.65, f32[2,2,4,768]{3,1,2,0:T(2,128)S(1)} %copy.64, bf16[2,768,4,128]{1,3,2,0:T(8,128)(2,1)} %copy.59), kind=kOutput, calls=%fused_computation.18 | convolution fusion | flops 2417491968 | bytes 5816320 | tf_op jit(solution)/shard_map/bjhld,bhle->bjhde/dot_general | solution.py:65
  190.9 1.3 copy.66
  192.4 0.2 slice_reduce_fusion.2
  192.6 12.8 %all-gather.2 = f32[16,2,4]{2,1,0:T(2,128)S(1)} all-gather(f32[2,2,4]{2,1,0:T(2,128)S(1)} %copy.68), channel_id=4, replica_groups=mesh['sp'=8,'tp'=4] {'sp'}, dimensions={0}, use_global_device_ids=true | all-gather | bytes 576 | tf_op jit(solution)/shard_map/all_gather | solution.py:67
  205.4 0.1 fusion.32
  205.5 14.4 %all-gather.3 = f32[16,2,4]{2,1,0:T(2,128)S(1)} all-gather(f32[2,2,4]{2,1,0:T(2,128)S(1)} %copy.70), channel_id=5, replica_groups=mesh['sp'=8,'tp'=4] {'sp'}, dimensions={0}, use_global_device_ids=true | all-gather | bytes 576 | tf_op jit(solution)/shard_map/all_gather | solution.py:10
  219.9 3.8 %multiply_reduce_fusion = f32[2,2,4,128]{3,1,2,0:T(2,128)S(1)} fusion(f32[2,4,768,128]{3,2,1,0:T(8,128)} %copy.65, f32[2,2,4,768]{3,1,2,0:T(2,128)S(1)} %copy.64), kind=kLoop, calls=%fused_computation.8 | loop fusion | flops 3143680 | bytes 3203072 | tf_op jit(solution)/shard_map/reduce_sum | solution.py:66
  223.7 14.5 %all-gather.1 = f32[16,2,4,128]{3,2,1,0:T(4,128)S(1)} all-gather(f32[2,2,4,128]{3,2,1,0:T(4,128)S(1)} %copy.67), channel_id=3, replica_groups=mesh['sp'=8,'tp'=4] {'sp'}, dimensions={0}, use_global_device_ids=true | all-gather | bytes 73728 | tf_op jit(solution)/shard_map/all_gather | solution.py:10
  238.3 36.6 %all-gather.9.cloned.1.call-done = f32[16,2,4,128,128]{4,3,2,1,0:T(8,128)} async-done(((f32[2,2,4,128,128]{4,3,2,1,0:T(8,128)}), f32[16,2,4,128,128]{4,3,2,1,0:T(8,128)}) %all-gather.9.cloned.1.call-update) | async-done | bytes 8388624 | tf_op jit(solution)/shard_map/all_gather | solution.py:10
  274.9 1.3 slice.88
  276.2 11.2 %while.19 = (s32[]{:T(128)}, f32[2,2,4,128,128]{4,3,2,1,0:T(8,128)S(1)}, f32[2,2,4,128]{3,2,1,0:T(4,128)S(1)}, f32[2,2,4]{2,1,0:T(2,128)S(1)}, f32[8,2,2,4]{3,2,...) while((s32[]{:T(128)}, ...), condition=%wide.region_8.9_spmd, body=%wide.region_7.8_spmd.sunk | while | flops 792629 | bytes 3171159 | solution.py:16
  276.3 0.1 fusion.47
  276.4 1.4 fusion.46
  277.9 0.1 fusion.47
  278.0 1.4 fusion.46
  279.5 0.1 fusion.47
  279.6 1.4 fusion.46
  281.2 1.4 fusion.46
  282.8 1.4 fusion.46
  284.4 1.4 fusion.46
  286.0 1.4 fusion.46
  287.4 0.6 copy.81
  288.0 0.2 multiply_convert_fusion
  288.3 0.5 fusion.16
  288.8 0.4 fusion.14
  289.1 0.9 copy.82
  (65 shorter events, 1.5 us)
Async XLA Ops:
  7.2 1.6 copy-start
  7.2 127.8 %all-gather.7.cloned.1.call-start = ((), (), s32[]{:S(2)}) async-start(), calls=%async_computation | async-start | bytes 15728640 | tf_op jit(solution)/shard_map/all_gather | solution.py:39
  7.9 267.0 %all-gather.9.cloned.1.call-start = ((), (), s32[]{:S(2)}) async-start(), calls=%async_computation.1 | async-start | bytes 9437184 | tf_op jit(solution)/shard_map/all_gather | solution.py:10
  135.0 14.2 %copy-start.3 = (f32[2,4,4,768]{3,2,1,0:T(4,128)S(1)}, f32[2,4,4,768]{3,2,1,0:T(4,128)}, u32[]{:S(2)}) copy-start(f32[2,4,4,768]{3,2,1,0:T(4,128)} %param.14) | copy-start | bytes 294916
  149.6 11.9 %copy-start.5 = (bf16[4096,512]{1,0:T(8,128)(2,1)S(1)}, bf16[4096,512]{1,0:T(8,128)(2,1)}, u32[]{:S(2)}) copy-start(bf16[4096,512]{1,0:T(8,128)(2,1)} %param.10) | copy-start | bytes 12582916
  185.6 6.7 %copy-start.1 = (bf16[2,128,512]{2,1,0:T(8,128)(2,1)S(1)}, bf16[2,128,512]{2,1,0:T(8,128)(2,1)}, u32[]{:S(2)}) copy-start(bf16[2,128,512]{2,1,0:T(8,128)(2,1)} %param.15) | copy-start | bytes 786436
  288.2 1.8 copy-start.2
  288.3 1.7 copy-start.4
Sparse Core Ops, SparseCore 0:
  9.8 125.0 all-gather.6
  192.3 82.5 all-gather.8
where the time goes:
time: 298 us; the launch traced here: 297 us
  waiting for transfers between devices  163 us (55%)
  blocking collectives  41.7 us (14%)
  matrix products  36.8 us (12%)
  other arithmetic  21 us (7%)
  local copies, waits for them, and re-layouts  20 us (7%)
  between operations  14.3 us (5%)
    all_gather x1, waiting for transfers between devices, on_device(): piece = lax.all_gather(tokens, 'tp', axis=2, tiled=True)  125 us
    all_gather x1, waiting for transfers between devices, combined_all(): everything = jax.tree.map(lambda part: lax.all_gather(part, axis), array)  36.6 us
    all_gather x2, blocking collectives, combined_all(): everything = jax.tree.map(lambda part: lax.all_gather(part, axis), array)  28.9 us
    all_gather x1, blocking collectives, on_device(): every_total = lax.all_gather(totals[None], 'sp', axis=0, tiled=True)  12.8 us
    dot_general x1, matrix products, on_device(): value_sum = jnp.dot(flat_piece, w_value, preferred_element_type=jnp.float32)  11.9 us
    dot_general x1, matrix products, on_device(): key_sum = jnp.dot(flat_piece, w_key, preferred_element_type=jnp.float32)  10.8 us
    add x7, other arithmetic, joint_max(): memory_a * carried[..., None, None] + memory_b * own_part[..., None, None]  10.1 us
    mul x2, local copies, waits for them, and re-layouts, on_device(): key_f = key_rows.astype(jnp.float32).transpose(0, 2, 1, 3) * HEAD ** (-0.5)  8.72 us
  transfers between devices with their start and end apart: 2, of which 2 were waited for; matrix products, arithmetic and copies ran while one was open for 2% of the time, Pallas kernels for 0%

commit v1 on v0

--- a/solution.py
+++ b/solution.py
@@ -36,7 +36,7 @@
         w_gate.shape[0], 4 * per_head
     )
     bias_own = lax.dynamic_slice_in_dim(forget_bias, first_head, per_head, 1)
-    piece = lax.all_gather(tokens, "tp", axis=2, tiled=True)
+    piece = jnp.concatenate(lax.all_gather(tokens, "tp"), axis=2)
     piece_width = piece.shape[2]
     flat_piece = piece.reshape(row_count, piece_width)
     key_sum = jnp.dot(flat_piece, w_key, preferred_element_type=jnp.float32)

time: 298 us -> 320 us (1.074)
  local copies, waits for them, and re-layouts: 20 us -> 45.8 us
  matrix products: 36.8 us -> 33.3 us
    all_gather x0 -> x1, local copies, waits for them, and re-layouts: none -> 16.2 us  [on_device(): piece = jnp.concatenate(lax.all_gather(tokens, 'tp'), axis=2)]
    unnamed x14 -> x17, local copies, waits for them, and re-layouts: 1.46 us -> 11 us
    dot_general x1, matrix products: 7.95 us -> 3.34 us  [on_device(): jnp.dot(flat_piece, gate_cols, preferred_element_type=jnp.float32)]
where the time goes in v1:
time: 320 us; the launch traced here: 319 us
  waiting for transfers between devices  161 us (50%)
  local copies, waits for them, and re-layouts  45.8 us (14%)
  blocking collectives  42.8 us (13%)
  matrix products  33.3 us (10%)
  other arithmetic  21 us (7%)
  between operations  14.3 us (4%)
    all_gather x1, waiting for transfers between devices, on_device(): piece = jnp.concatenate(lax.all_gather(tokens, 'tp'), axis=2)  125 us
    all_gather x1, waiting for transfers between devices, combined_all(): everything = jax.tree.map(lambda part: lax.all_gather(part, axis), array)  35.5 us
    all_gather x2, blocking collectives, combined_all(): everything = jax.tree.map(lambda part: lax.all_gather(part, axis), array)  27.9 us
    all_gather x1, local copies, waits for them, and re-layouts, on_device(): piece = jnp.concatenate(lax.all_gather(tokens, 'tp'), axis=2)  16.2 us
    all_gather x1, blocking collectives, on_device(): every_total = lax.all_gather(totals[None], 'sp', axis=0, tiled=True)  14.9 us
    dot_general x1, matrix products, on_device(): key_sum = jnp.dot(flat_piece, w_key, preferred_element_type=jnp.float32)  12 us
    dot_general x1, matrix products, on_device(): value_sum = jnp.dot(flat_piece, w_value, preferred_element_type=jnp.float32)  11.7 us
    unnamed x17, local copies, waits for them, and re-layouts  11 us
  transfers between devices with their start and end apart: 2, of which 2 were waited for; matrix products, arithmetic and copies ran while one was open for 2% of the time, Pallas kernels for 0%

profile of v1, /device:TPU:0, one launch (start us, length us, event | category | flops | bytes accessed | tf_op | source)
XLA Modules:
  0.0 318.8 jit_solution(14364375979871126477)
XLA Ops:
  7.2 0.7 all-gather.8.cloned.1.call-update
  8.0 0.2 copy-done
  8.3 0.8 fusion.34
  9.1 0.8 constant_dynamic-slice_fusion
  9.9 125.1 %all-gather.8.cloned.1.call-done = bf16[8,768,1024]{2,1,0:T(8,128)(2,1)} async-done(((bf16[2,768,1024]{2,1,0:T(8,128)(2,1)}), bf16[8,768,1024]{2,1,0:T(8,128)(2,1)}) %all-gather.8.cloned.1.call-update) | async-done | bytes 12582928 | tf_op jit(solution)/shard_map/all_gather | solution.py:39
  135.0 16.2 %copy.61 = bf16[4,2,768,1024]{3,0,2,1:T(4,128)(2,1)S(1)} copy(bf16[4,2,768,1024]{3,2,1,0:T(8,128)(2,1)} %bitcast.99) | data formatting | bytes 25165824 | tf_op jit(solution)/shard_map/all_gather | solution.py:39
  151.1 4.7 %copy.97 = bf16[192,8,4,1024]{3,1,2,0:T(8,128)(2,1)S(1)} copy(bf16[192,8,4,1024]{3,2,1,0:T(4,128)(2,1)S(1)} %bitcast.98) | data formatting | bytes 25165824
  155.8 4.6 %copy-done.2 = bf16[192,8,4,1024]{3,1,2,0:T(8,128)(2,1)} copy-done((bf16[192,8,4,1024]{3,1,2,0:T(8,128)(2,1)}, bf16[192,8,4,1024]{3,1,2,0:T(8,128)(2,1)S(1)}, u32[]{:S(2)}) %copy-start.2) | copy-done | bytes 12582936
  160.4 3.3 %convolution_bitcast_fusion = f32[1536,16]{0,1:T(8,128)S(1)} fusion(bf16[4096,16]{0,1:T(8,128)(2,1)S(1)} %reshape.198, bf16[1536,4096]{1,0:T(8,128)(2,1)S(1)} %bitcast.95), kind=kOutput, calls=%fused_computation.16 | convolution fusion | flops 201326592 | bytes 12812288 | tf_op jit(solution)/shard_map/dot_general | solution.py:44
  163.9 0.1 fusion.22
  164.0 2.3 reduce-window.14
  166.3 0.2 slice_reduce_fusion.1
  166.5 0.4 reduce-window.15
  167.0 12.0 %convert_multiply_fusion = f32[1536,512]{1,0:T(8,128)} fusion(bf16[1536,4096]{1,0:T(8,128)(2,1)} %bitcast.96, bf16[4096,512]{1,0:T(8,128)(2,1)} %param.10), kind=kOutput, calls=%fused_computation.12 | convolution fusion | flops 6444810240 | bytes 19922944 | tf_op jit(solution)/shard_map/dot_general | solution.py:42
  179.0 4.9 %mul.152 = f32[2,768,4,128]{3,2,1,0:T(4,128)} reshape(f32[1536,512]{1,0:T(8,128)} %convert_multiply_fusion) | data formatting | bytes 6291456 | tf_op jit(solution)/shard_map/mul | solution.py:62
  183.9 3.8 %copy.68 = f32[2,4,768,128]{3,2,1,0:T(8,128)} copy(f32[2,4,768,128]{3,1,2,0:T(4,128)} %bitcast.100) | data formatting | bytes 6291456 | tf_op jit(solution)/shard_map/mul | solution.py:62
  187.7 0.2 slice_reduce_fusion.3
  187.8 2.3 reduce-window.16
  190.1 0.2 slice_reduce_fusion
  190.2 0.4 reduce-window.19
  190.7 0.1 fusion.30
  190.8 0.1 fusion.25
  190.9 0.1 subtract_exponential_fusion.1
  191.1 11.7 %convolution_convert_fusion.1 = bf16[1536,512]{1,0:T(8,128)(2,1)} fusion(bf16[1536,4096]{1,0:T(8,128)(2,1)} %bitcast.97, bf16[4096,512]{1,0:T(8,128)(2,1)} %param.11), kind=kOutput, calls=%fused_computation.15 | convolution fusion | flops 6443237376 | bytes 18350080 | tf_op jit(solution)/shard_map/dot_general | solution.py:43
  202.8 2.4 reshape.197
  205.2 2.3 copy.62
  207.5 5.3 %fusion.8 = f32[2,2,4,128,128]{3,4,1,2,0:T(8,128)S(1)} fusion(f32[2,4,768,128]{3,2,1,0:T(8,128)} %copy.68, f32[2,2,4,768]{3,1,2,0:T(2,128)S(1)} %copy.67, bf16[2,768,4,128]{1,3,2,0:T(8,128)(2,1)} %copy.62), kind=kOutput, calls=%fused_computation.18 | convolution fusion | flops 2417491968 | bytes 5816320 | tf_op jit(solution)/shard_map/bjhld,bhle->bjhde/dot_general | solution.py:65
  212.8 1.4 copy.69
  214.4 3.8 %multiply_reduce_fusion = f32[2,2,4,128]{3,1,2,0:T(2,128)S(1)} fusion(f32[2,4,768,128]{3,2,1,0:T(8,128)} %copy.68, f32[2,2,4,768]{3,1,2,0:T(2,128)S(1)} %copy.67), kind=kLoop, calls=%fused_computation.8 | loop fusion | flops 3143680 | bytes 3203072 | tf_op jit(solution)/shard_map/reduce_sum | solution.py:66
  218.2 14.5 %all-gather.2 = f32[16,2,4,128]{3,2,1,0:T(4,128)S(1)} all-gather(f32[2,2,4,128]{3,2,1,0:T(4,128)S(1)} %copy.70), channel_id=4, replica_groups=mesh['sp'=8,'tp'=4] {'sp'}, dimensions={0}, use_global_device_ids=true | all-gather | bytes 73728 | tf_op jit(solution)/shard_map/all_gather | solution.py:10
  232.8 0.2 slice_reduce_fusion.2
  232.9 14.9 %all-gather.3 = f32[16,2,4]{2,1,0:T(2,128)S(1)} all-gather(f32[2,2,4]{2,1,0:T(2,128)S(1)} %copy.71), channel_id=5, replica_groups=mesh['sp'=8,'tp'=4] {'sp'}, dimensions={0}, use_global_device_ids=true | all-gather | bytes 576 | tf_op jit(solution)/shard_map/all_gather | solution.py:67
  247.9 13.4 %all-gather.4 = f32[16,2,4]{2,1,0:T(2,128)S(1)} all-gather(f32[2,2,4]{2,1,0:T(2,128)S(1)} %copy.73), channel_id=6, replica_groups=mesh['sp'=8,'tp'=4] {'sp'}, dimensions={0}, use_global_device_ids=true | all-gather | bytes 576 | tf_op jit(solution)/shard_map/all_gather | solution.py:10
  261.4 35.5 %all-gather.10.cloned.1.call-done = f32[16,2,4,128,128]{4,3,2,1,0:T(8,128)} async-done(((f32[2,2,4,128,128]{4,3,2,1,0:T(8,128)}), f32[16,2,4,128,128]{4,3,2,1,0:T(8,128)}) %all-gather.10.cloned.1.call-update) | async-done | bytes 8388624 | tf_op jit(solution)/shard_map/all_gather | solution.py:10
  296.9 1.3 slice.88
  298.2 11.1 %while.19 = (s32[]{:T(128)}, f32[2,2,4,128,128]{4,3,2,1,0:T(8,128)S(1)}, f32[2,2,4,128]{3,2,1,0:T(4,128)S(1)}, f32[2,2,4]{2,1,0:T(2,128)S(1)}, f32[8,2,2,4]{3,2,...) while((s32[]{:T(128)}, ...), condition=%wide.region_8.9_spmd, body=%wide.region_7.8_spmd.sunk | while | flops 792629 | bytes 3171167 | solution.py:16
  298.2 1.4 fusion.46
  299.8 1.4 fusion.46
  301.4 1.4 fusion.46
  303.0 1.4 fusion.46
  304.5 1.4 fusion.46
  306.1 1.4 fusion.46
  307.7 1.4 fusion.46
  309.3 0.2 multiply_convert_fusion
  309.5 0.7 copy.84
  310.2 0.5 fusion.16
  310.7 0.4 fusion.14
  311.1 0.9 copy.85
  (69 shorter events, 1.8 us)
Async XLA Ops:
  7.2 1.1 copy-start
  7.2 127.8 %all-gather.8.cloned.1.call-start = ((), (), s32[]{:S(2)}) async-start(), calls=%async_computation | async-start | bytes 15728640 | tf_op jit(solution)/shard_map/all_gather | solution.py:39
  7.9 289.0 %all-gather.10.cloned.1.call-start = ((), (), s32[]{:S(2)}) async-start(), calls=%async_computation.1 | async-start | bytes 9437184 | tf_op jit(solution)/shard_map/all_gather | solution.py:10
  155.8 4.6 %copy-start.2 = (bf16[192,8,4,1024]{3,1,2,0:T(8,128)(2,1)}, bf16[192,8,4,1024]{3,1,2,0:T(8,128)(2,1)S(1)}, u32[]{:S(2)}) copy-start(bf16[192,8,4,1024]{3,1,2,0:T(8,128)(2,1)S(1)} %copy.97) | copy-start | bytes 37748740
  183.9 6.8 %copy-start.5 = (f32[2,4,4,768]{3,2,1,0:T(4,128)S(1)}, f32[2,4,4,768]{3,2,1,0:T(4,128)}, u32[]{:S(2)}) copy-start(f32[2,4,4,768]{3,2,1,0:T(4,128)} %param.14) | copy-start | bytes 294916
  207.5 6.8 %copy-start.3 = (bf16[2,128,512]{2,1,0:T(8,128)(2,1)S(1)}, bf16[2,128,512]{2,1,0:T(8,128)(2,1)}, u32[]{:S(2)}) copy-start(bf16[2,128,512]{2,1,0:T(8,128)(2,1)} %param.15) | copy-start | bytes 786436
  309.2 2.7 copy-start.1
  309.4 2.5 copy-start.4
  309.5 2.4 copy-start.6
Sparse Core Ops, SparseCore 0:
  9.8 125.0 all-gather.7
  214.3 82.5 all-gather.9
